TPU v7x, 32 devices: a whole 2x2x4 slice. The times are simulated.
32 devices in a mesh: fs: 8 (over z, y), tp: 4 (over x, core).
Axes of the slice: x: 2, y: 2, z: 4, core: 2. Of those that a mesh axis runs over, the one named last changes fastest.
Arguments:
- saved_input: bfloat16 [16384, 2048], P('fs'), may hold values from -6 to 6
- query_cotangent: bfloat16 [16384, 2048], P('fs', 'tp'), may hold values from -0.046875 to 0.046875
- forget_cotangent: bfloat16 [16384, 2048], P('fs', 'tp'), may hold values from -0.046875 to 0.046875
- mixed_output: bfloat16 [16384, 2048], P('fs', 'tp'), may hold values from -6 to 6
- out_cotangent: bfloat16 [16384, 2048], P('fs'), may hold values from -0.046875 to 0.046875
- query_basis: bfloat16 [2048, 256], replicated, may hold values from -0.125 to 0.125
- forget_basis: bfloat16 [2048, 256], replicated, may hold values from -0.125 to 0.125
- out_basis: bfloat16 [2048, 256], replicated, may hold values from -0.125 to 0.125
- query_weight: float32 [2048, 2048], P('fs', 'tp'), may hold values from -0.125 to 0.125
- forget_weight: float32 [2048, 2048], P('fs', 'tp'), may hold values from -0.125 to 0.125
- out_weight: float32 [2048, 2048], P('fs', 'tp'), may hold values from -0.125 to 0.125
- query_first: float32 [256, 2048], P('fs', 'tp'), may hold values from -25 to 25
- forget_first: float32 [256, 2048], P('fs', 'tp'), may hold values from -25 to 25
- out_first: float32 [256, 2048], P('fs', 'tp'), may hold values from -25 to 25
- query_second: float32 [256, 2048], P('fs', 'tp'), may hold values from 0.2 to 2
- forget_second: float32 [256, 2048], P('fs', 'tp'), may hold values from 0.2 to 2
- out_second: float32 [256, 2048], P('fs', 'tp'), may hold values from 0.2 to 2
Outputs:
- query_update: float32 [2048, 2048], P('fs', 'tp')
- forget_update: float32 [2048, 2048], P('fs', 'tp')
- out_update: float32 [2048, 2048], P('fs', 'tp')
- query_first_new: float32 [256, 2048], P('fs', 'tp')
- forget_first_new: float32 [256, 2048], P('fs', 'tp')
- out_first_new: float32 [256, 2048], P('fs', 'tp')
- query_second_new: float32 [256, 2048], P('fs', 'tp')
- forget_second_new: float32 [256, 2048], P('fs', 'tp')
- out_second_new: float32 [256, 2048], P('fs', 'tp')
- query_copy: bfloat16 [2048, 2048], P(None, 'tp')
- forget_copy: bfloat16 [2048, 2048], P(None, 'tp')
- out_copy: bfloat16 [2048, 2048], P(None, 'tp')
All inputs are finite; a program needn't handle non-finite values.
Results may differ from a plain program's by a relative error of at most 0.0065.
Values may be sent and summed in bfloat16 or wider, within the bound.
A program may use at most 128 MiB of HBM per device.

v0:
```python
import jax
import jax.numpy as jnp
from jax import lax
from jax.sharding import PartitionSpec as P

WIDTH = 2048
RANK = 256
highest = lax.Precision.HIGHEST


def contract_rows(left, right):
    return lax.dot_general(
        left, right, (((0,), (0,)), ((), ())), precision=None, preferred_element_type=jnp.float32
    )


def moments(source, cotangent, basis, weight, first, second):
    row_count = weight.shape[0]
    basis_rows = lax.dynamic_slice_in_dim(
        basis, lax.axis_index("fs") * row_count, row_count, 0
    ).astype(jnp.float32)
    reduced = jnp.dot(source, basis, preferred_element_type=jnp.float32)
    reduced_high = reduced.astype(jnp.bfloat16)
    reduced_low = (reduced - reduced_high.astype(jnp.float32)).astype(jnp.bfloat16)
    projected = lax.psum_scatter(
        (contract_rows(reduced_high, cotangent) + contract_rows(reduced_low, cotangent)).astype(
            jnp.bfloat16
        ),
        "fs",
        scatter_dimension=0,
        tiled=True,
    ).astype(jnp.float32)
    first_new = 0.8 * first + 0.2 * projected
    second_new = 0.95 * second + 0.05 * projected * projected
    direction = first_new / (jnp.sqrt(second_new) + 1e-08)
    return (direction, first_new, second_new, jnp.sum(direction * direction), basis_rows)


def expand(direction, basis_rows, total, weight):
    stepped = jnp.dot(
        basis_rows, lax.all_gather(direction, "fs", axis=0, tiled=True), precision=highest
    )
    update = stepped * lax.rsqrt(total / (RANK * WIDTH) + 1e-06)
    return (update, (weight - 0.05 * update).astype(jnp.bfloat16))


def local(
    saved_input,
    query_cotangent,
    forget_cotangent,
    mixed_output,
    out_cotangent,
    query_basis,
    forget_basis,
    out_basis,
    query_weight,
    forget_weight,
    out_weight,
    query_first,
    forget_first,
    out_first,
    query_second,
    forget_second,
    out_second,
):
    query_dir, query_one, query_two, query_sq, query_rows = moments(
        saved_input, query_cotangent, query_basis, query_weight, query_first, query_second
    )
    forget_dir, forget_one, forget_two, forget_sq, forget_rows = moments(
        saved_input, forget_cotangent, forget_basis, forget_weight, forget_first, forget_second
    )
    out_dir, out_one, out_two, out_sq, out_rows = moments(
        out_cotangent, mixed_output, out_basis, out_weight, out_first, out_second
    )
    totals = lax.psum((query_sq, forget_sq, out_sq), ("fs", "tp"))
    query_step, query_new = expand(query_dir, query_rows, totals[0], query_weight)
    forget_step, forget_new = expand(forget_dir, forget_rows, totals[1], forget_weight)
    out_step, out_new = expand(out_dir, out_rows, totals[2], out_weight)
    query_copy, forget_copy, out_copy = (
        lax.all_gather(query_new, "fs", axis=0, tiled=True),
        lax.all_gather(forget_new, "fs", axis=0, tiled=True),
        lax.all_gather(out_new, "fs", axis=0, tiled=True),
    )
    return (
        query_step,
        forget_step,
        out_step,
        query_one,
        forget_one,
        out_one,
        query_two,
        forget_two,
        out_two,
        query_copy,
        forget_copy,
        out_copy,
    )


def solution(mesh):
    in_specs = (
        P("fs", None),
        P("fs", "tp"),
        P("fs", "tp"),
        P("fs", "tp"),
        P("fs", None),
        P(),
        P(),
        P(),
        P("fs", "tp"),
        P("fs", "tp"),
        P("fs", "tp"),
        P("fs", "tp"),
        P("fs", "tp"),
        P("fs", "tp"),
        P("fs", "tp"),
        P("fs", "tp"),
        P("fs", "tp"),
    )
    out_specs = (
        P("fs", "tp"),
        P("fs", "tp"),
        P("fs", "tp"),
        P("fs", "tp"),
        P("fs", "tp"),
        P("fs", "tp"),
        P("fs", "tp"),
        P("fs", "tp"),
        P("fs", "tp"),
        P(None, "tp"),
        P(None, "tp"),
        P(None, "tp"),
    )
    return jax.shard_map(local, mesh=mesh, in_specs=in_specs, out_specs=out_specs, check_vma=False)
```

profile of v0, /device:TPU:0, one launch (start us, length us, event | category | flops | bytes accessed | tf_op | source)
XLA Modules:
  0.0 426.3 jit_solution(11486083367784151921)
XLA Ops:
  7.2 6.2 %fusion.31 = f32[2048,256]{1,0:T(8,128)S(1)} fusion(bf16[2048,2048]{1,0:T(8,128)(2,1)} %param.17, bf16[2048,256]{1,0:T(8,128)(2,1)} %param.23), kind=kOutput, calls=%fused_computation.49 | convolution fusion | flops 2147483648 | bytes 11534336 | tf_op jit(solution)/shard_map/dot_general | solution.py:22
  14.3 1.5 fusion.1
  15.9 6.0 %fusion.32 = f32[2048,256]{1,0:T(8,128)S(1)} fusion(bf16[2048,2048]{1,0:T(8,128)(2,1)} %param.21, bf16[2048,256]{1,0:T(8,128)(2,1)S(1)} %copy-done.13), kind=kOutput, calls=%fused_computation.50 | convolution fusion | flops 2147483648 | bytes 11534336 | tf_op jit(solution)/shard_map/dot_general | solution.py:22
  22.6 1.4 fusion.2
  24.2 6.0 %fusion.30 = f32[2048,256]{1,0:T(8,128)S(1)} fusion(bf16[2048,2048]{1,0:T(8,128)(2,1)} %param.17, bf16[2048,256]{1,0:T(8,128)(2,1)S(1)} %copy-done.14), kind=kOutput, calls=%fused_computation.48 | convolution fusion | flops 2147483648 | bytes 11534336 | tf_op jit(solution)/shard_map/dot_general | solution.py:22
  31.1 1.5 fusion
  32.6 48.1 %reduce-scatter.6.cloned.1.call-done = bf16[32,512]{1,0:T(8,128)(2,1)} async-done(((bf16[256,512]{1,0:T(8,128)(2,1)}), bf16[32,512]{1,0:T(8,128)(2,1)}) %reduce-scatter.6.cloned.1.call-update) | async-done | bytes 32784 | tf_op jit(solution)/shard_map/reduce_scatter | solution.py:25
  80.8 2.0 multiply_reduce_fusion.1
  82.8 31.7 %all_gather.19 = f32[256,512]{1,0:T(8,128)S(1)} all-gather(f32[32,512]{1,0:T(8,128)S(1)} %get-tuple-element.20), channel_id=1, replica_groups=mesh['fs'=8,'tp'=4] {'fs'}, dimensions={0}, use_global_device_ids=true | all-gather | bytes 589824 | tf_op jit(solution)/shard_map/all_gather | solution.py:41
  114.5 31.3 %reduce-scatter.8.cloned.1.call-done = bf16[32,512]{1,0:T(8,128)(2,1)} async-done(((bf16[256,512]{1,0:T(8,128)(2,1)}), bf16[32,512]{1,0:T(8,128)(2,1)}) %reduce-scatter.8.cloned.1.call-update) | async-done | bytes 32784 | tf_op jit(solution)/shard_map/reduce_scatter | solution.py:25
  145.8 2.0 multiply_reduce_fusion
  147.9 63.0 %reduce-scatter.4.cloned.1.call-done = bf16[32,512]{1,0:T(8,128)(2,1)} async-done(((bf16[256,512]{1,0:T(8,128)(2,1)}), bf16[32,512]{1,0:T(8,128)(2,1)}) %reduce-scatter.4.cloned.1.call-update) | async-done | bytes 32784 | tf_op jit(solution)/shard_map/reduce_scatter | solution.py:25
  210.9 2.0 multiply_reduce_fusion.2
  212.9 40.4 %all-reduce = (f32[]{:T(128)}, f32[]{:T(128)}, f32[]{:T(128)}) all-reduce(f32[]{:T(128)} %get-tuple-element.23, f32[]{:T(128)} %get-tuple-element.19, f32[]{:T(128)} %get-tuple-element.15), channel_id=1, replica_groups=mesh['fs'=8,'tp'=4] {'fs','tp'}, use_global_device_ids=true, to_apply=%region_2.0 | all-reduce | flops 3 | bytes 24 | tf_op jit(solution)/shard_map/psum | solution.py:75
  254.0 2.3 subtract_convert_fusion.7
  257.1 32.5 %all_gather.20 = f32[256,512]{1,0:T(8,128)S(1)} all-gather(f32[32,512]{1,0:T(8,128)S(1)} %get-tuple-element.16), channel_id=1, replica_groups=mesh['fs'=8,'tp'=4] {'fs'}, dimensions={0}, use_global_device_ids=true | all-gather | bytes 589824 | tf_op jit(solution)/shard_map/all_gather | solution.py:41
  289.6 2.5 subtract_convert_fusion.6
  292.8 32.1 %all_gather.18 = f32[256,512]{1,0:T(8,128)S(1)} all-gather(f32[32,512]{1,0:T(8,128)S(1)} %get-tuple-element.24), channel_id=1, replica_groups=mesh['fs'=8,'tp'=4] {'fs'}, dimensions={0}, use_global_device_ids=true | all-gather | bytes 589824 | tf_op jit(solution)/shard_map/all_gather | solution.py:41
  324.9 2.3 subtract_convert_fusion.8
  327.2 35.1 %all-gather.8.cloned.1.call-done = bf16[2048,512]{1,0:T(8,128)(2,1)} async-done(((bf16[256,512]{1,0:T(8,128)(2,1)}), bf16[2048,512]{1,0:T(8,128)(2,1)}) %all-gather.8.cloned.1.call-update) | async-done | bytes 2097168 | tf_op jit(solution)/shard_map/all_gather | solution.py:82
  362.4 50.2 %all-gather.4.cloned.1.call-done = bf16[2048,512]{1,0:T(8,128)(2,1)} async-done(((bf16[256,512]{1,0:T(8,128)(2,1)}), bf16[2048,512]{1,0:T(8,128)(2,1)}) %all-gather.4.cloned.1.call-update) | async-done | bytes 2097168 | tf_op jit(solution)/shard_map/all_gather | solution.py:80
  412.6 3.2 copy.32
  415.8 1.3 copy.33
  418.1 1.3 copy.34
  (46 shorter events, 3.7 us)
Async XLA Ops:
  7.2 6.3 %copy-start = (bf16[2048,512]{1,0:T(8,128)(2,1)S(1)}, bf16[2048,512]{1,0:T(8,128)(2,1)}, u32[]{:S(2)}) copy-start(bf16[2048,512]{1,0:T(8,128)(2,1)} %param.19) | copy-start | bytes 6291460
  7.2 73.6 %reduce-scatter.6.cloned.1.call-start = ((), (), s32[]{:S(2)}) async-start(), calls=%async_computation.4 | async-start | bytes 294912 | tf_op jit(solution)/shard_map/reduce_scatter | solution.py:25
  14.3 1.6 copy-start.13
  15.8 130.0 %reduce-scatter.8.cloned.1.call-start = ((), (), s32[]{:S(2)}) async-start(), calls=%async_computation.5 | async-start | bytes 294912 | tf_op jit(solution)/shard_map/reduce_scatter | solution.py:25
  15.8 6.0 %copy-start.1 = (bf16[2048,512]{1,0:T(8,128)(2,1)S(1)}, bf16[2048,512]{1,0:T(8,128)(2,1)}, u32[]{:S(2)}) copy-start(bf16[2048,512]{1,0:T(8,128)(2,1)} %param.20) | copy-start | bytes 6291460
  22.6 1.5 copy-start.14
  24.1 186.8 %reduce-scatter.4.cloned.1.call-start = ((), (), s32[]{:S(2)}) async-start(), calls=%async_computation.3 | async-start | bytes 294912 | tf_op jit(solution)/shard_map/reduce_scatter | solution.py:25
  24.2 6.1 %copy-start.2 = (bf16[2048,512]{1,0:T(8,128)(2,1)S(1)}, bf16[2048,512]{1,0:T(8,128)(2,1)}, u32[]{:S(2)}) copy-start(bf16[2048,512]{1,0:T(8,128)(2,1)} %param.18) | copy-start | bytes 6291460
  31.0 49.8 %copy-start.7 = (f32[32,512]{1,0:T(8,128)S(1)}, f32[32,512]{1,0:T(8,128)}, u32[]{:S(2)}) copy-start(f32[32,512]{1,0:T(8,128)} %param.32) | copy-start | bytes 196612
  31.0 49.8 %copy-start.8 = (f32[32,512]{1,0:T(8,128)S(1)}, f32[32,512]{1,0:T(8,128)}, u32[]{:S(2)}) copy-start(f32[32,512]{1,0:T(8,128)} %param.29) | copy-start | bytes 196612
  31.0 114.8 %copy-start.9 = (f32[32,512]{1,0:T(8,128)S(1)}, f32[32,512]{1,0:T(8,128)}, u32[]{:S(2)}) copy-start(f32[32,512]{1,0:T(8,128)} %param.33) | copy-start | bytes 196612
  31.0 114.8 %copy-start.10 = (f32[32,512]{1,0:T(8,128)S(1)}, f32[32,512]{1,0:T(8,128)}, u32[]{:S(2)}) copy-start(f32[32,512]{1,0:T(8,128)} %param.30) | copy-start | bytes 196612
  31.0 179.8 %copy-start.11 = (f32[32,512]{1,0:T(8,128)S(1)}, f32[32,512]{1,0:T(8,128)}, u32[]{:S(2)}) copy-start(f32[32,512]{1,0:T(8,128)} %param.31) | copy-start | bytes 196612
  31.1 179.8 %copy-start.12 = (f32[32,512]{1,0:T(8,128)S(1)}, f32[32,512]{1,0:T(8,128)}, u32[]{:S(2)}) copy-start(f32[32,512]{1,0:T(8,128)} %param.28) | copy-start | bytes 196612
  32.5 221.5 %copy-start.5 = (f32[256,512]{1,0:T(8,128)S(1)}, f32[256,512]{1,0:T(8,128)}, u32[]{:S(2)}) copy-start(f32[256,512]{1,0:T(8,128)} %param.26) | copy-start | bytes 1572868
  32.5 294.7 %all-gather.6.cloned.1.call-start = ((), (), s32[]{:S(2)}) async-start(), calls=%async_computation.7 | async-start | bytes 2359296 | tf_op jit(solution)/shard_map/all_gather | solution.py:81
  256.3 68.7 %copy-start.6 = (f32[256,512]{1,0:T(8,128)S(1)}, f32[256,512]{1,0:T(8,128)}, u32[]{:S(2)}) copy-start(f32[256,512]{1,0:T(8,128)} %param.25) | copy-start | bytes 1572868
  256.3 106.1 %all-gather.8.cloned.1.call-start = ((), (), s32[]{:S(2)}) async-start(), calls=%async_computation.8 | async-start | bytes 2359296 | tf_op jit(solution)/shard_map/all_gather | solution.py:82
  292.1 120.5 %all-gather.4.cloned.1.call-start = ((), (), s32[]{:S(2)}) async-start(), calls=%async_computation.6 | async-start | bytes 2359296 | tf_op jit(solution)/shard_map/all_gather | solution.py:80
  412.6 3.2 copy-start.3
  415.8 2.3 copy-start.4
Sparse Core Ops, SparseCore 0:
  15.9 64.7 reduce-scatter.5
  84.6 61.1 reduce-scatter.7
  149.7 61.1 reduce-scatter.3
  256.4 54.7 all-gather.5
  313.8 48.5 all-gather.7
  364.9 47.6 all-gather.3
where the time goes:
time: 427 us; the launch traced here: 426 us
  waiting for transfers between devices  228 us (53%)
  blocking collectives  137 us (32%)
  matrix products  31.9 us (7%)
  between operations  16.4 us (4%)
  local copies, waits for them, and re-layouts  6.94 us (2%)
  other arithmetic  6.12 us (1%)
    reduce_scatter x3, waiting for transfers between devices, moments(): lax.psum_scatter((contract_rows(reduced_high, cotangent) + contract_rows(...  142 us
    all_gather x3, blocking collectives, expand(): lax.all_gather(direction, 'fs', axis=0, tiled=True)  96.4 us
    all_gather x1, waiting for transfers between devices, local(): lax.all_gather(query_new, 'fs', axis=0, tiled=True)  50.2 us
    psum x1, blocking collectives, local(): totals = lax.psum((query_sq, forget_sq, out_sq), ('fs', 'tp'))  40.4 us
    all_gather x1, waiting for transfers between devices, local(): lax.all_gather(out_new, 'fs', axis=0, tiled=True)  35.1 us
    dot_general x3, matrix products, moments(): reduced = jnp.dot(source, basis, preferred_element_type=jnp.float32)  18.3 us
  transfers between devices with their start and end apart: 6, of which 5 were waited for; matrix products, arithmetic and copies ran while one was open for 6% of the time, Pallas kernels for 0%

commit v1 on v0

--- a/solution.py
+++ b/solution.py
@@ -72,7 +72,7 @@
     out_dir, out_one, out_two, out_sq, out_rows = moments(
         out_cotangent, mixed_output, out_basis, out_weight, out_first, out_second
     )
-    totals = lax.psum((query_sq, forget_sq, out_sq), ("fs", "tp"))
+    totals = lax.psum(lax.psum((query_sq, forget_sq, out_sq), "tp"), "fs")
     query_step, query_new = expand(query_dir, query_rows, totals[0], query_weight)
     forget_step, forget_new = expand(forget_dir, forget_rows, totals[1], forget_weight)
     out_step, out_new = expand(out_dir, out_rows, totals[2], out_weight)

time: 427 us -> 412 us (0.965)
  blocking collectives: 137 us -> 123 us
    psum x1 -> x2, blocking collectives: 40.4 us -> 26.3 us  [local(): totals = lax.psum(lax.psum((query_sq, forget_sq, out_sq), 'tp'), 'fs')]
where the time goes in v1:
time: 412 us
  waiting for transfers between devices  227 us (55%)
  blocking collectives  123 us (30%)
  matrix products  31.9 us (8%)
  between operations  16.4 us (4%)
  local copies, waits for them, and re-layouts  6.94 us (2%)
  other arithmetic  6.12 us (1%)
    reduce_scatter x3, waiting for transfers between devices, moments(): lax.psum_scatter((contract_rows(reduced_high, cotangent) + contract_rows(...  142 us
    all_gather x3, blocking collectives, expand(): lax.all_gather(direction, 'fs', axis=0, tiled=True)  96.5 us
    all_gather x1, waiting for transfers between devices, local(): lax.all_gather(query_new, 'fs', axis=0, tiled=True)  50.2 us
    all_gather x1, waiting for transfers between devices, local(): lax.all_gather(out_new, 'fs', axis=0, tiled=True)  34.7 us
    psum x2, blocking collectives, local(): totals = lax.psum(lax.psum((query_sq, forget_sq, out_sq), 'tp'), 'fs')  26.3 us
    dot_general x3, matrix products, moments(): reduced = jnp.dot(source, basis, preferred_element_type=jnp.float32)  18.3 us
  transfers between devices with their start and end apart: 6, of which 5 were waited for; matrix products, arithmetic and copies ran while one was open for 6% of the time, Pallas kernels for 0%

profile of v1, /device:TPU:0, one launch (start us, length us, event | category | flops | bytes accessed | tf_op | source)
XLA Modules:
  0.0 411.9 jit_solution(6063637765545253595)
XLA Ops:
  7.2 6.2 %fusion.31 = f32[2048,256]{1,0:T(8,128)S(1)} fusion(bf16[2048,2048]{1,0:T(8,128)(2,1)} %param.17, bf16[2048,256]{1,0:T(8,128)(2,1)} %param.23), kind=kOutput, calls=%fused_computation.49 | convolution fusion | flops 2147483648 | bytes 11534336 | tf_op jit(solution)/shard_map/dot_general | solution.py:22
  14.3 1.5 fusion.1
  15.9 6.0 %fusion.32 = f32[2048,256]{1,0:T(8,128)S(1)} fusion(bf16[2048,2048]{1,0:T(8,128)(2,1)} %param.21, bf16[2048,256]{1,0:T(8,128)(2,1)S(1)} %copy-done.13), kind=kOutput, calls=%fused_computation.50 | convolution fusion | flops 2147483648 | bytes 11534336 | tf_op jit(solution)/shard_map/dot_general | solution.py:22
  22.6 1.4 fusion.2
  24.2 6.0 %fusion.30 = f32[2048,256]{1,0:T(8,128)S(1)} fusion(bf16[2048,2048]{1,0:T(8,128)(2,1)} %param.17, bf16[2048,256]{1,0:T(8,128)(2,1)S(1)} %copy-done.14), kind=kOutput, calls=%fused_computation.48 | convolution fusion | flops 2147483648 | bytes 11534336 | tf_op jit(solution)/shard_map/dot_general | solution.py:22
  31.1 1.5 fusion
  32.6 48.1 %reduce-scatter.6.cloned.1.call-done = bf16[32,512]{1,0:T(8,128)(2,1)} async-done(((bf16[256,512]{1,0:T(8,128)(2,1)}), bf16[32,512]{1,0:T(8,128)(2,1)}) %reduce-scatter.6.cloned.1.call-update) | async-done | bytes 32784 | tf_op jit(solution)/shard_map/reduce_scatter | solution.py:25
  80.8 2.0 multiply_reduce_fusion.1
  82.8 31.7 %all_gather.19 = f32[256,512]{1,0:T(8,128)S(1)} all-gather(f32[32,512]{1,0:T(8,128)S(1)} %get-tuple-element.23), channel_id=1, replica_groups=mesh['fs'=8,'tp'=4] {'fs'}, dimensions={0}, use_global_device_ids=true | all-gather | bytes 589824 | tf_op jit(solution)/shard_map/all_gather | solution.py:41
  114.5 31.3 %reduce-scatter.8.cloned.1.call-done = bf16[32,512]{1,0:T(8,128)(2,1)} async-done(((bf16[256,512]{1,0:T(8,128)(2,1)}), bf16[32,512]{1,0:T(8,128)(2,1)}) %reduce-scatter.8.cloned.1.call-update) | async-done | bytes 32784 | tf_op jit(solution)/shard_map/reduce_scatter | solution.py:25
  145.8 2.0 multiply_reduce_fusion
  147.9 63.0 %reduce-scatter.4.cloned.1.call-done = bf16[32,512]{1,0:T(8,128)(2,1)} async-done(((bf16[256,512]{1,0:T(8,128)(2,1)}), bf16[32,512]{1,0:T(8,128)(2,1)}) %reduce-scatter.4.cloned.1.call-update) | async-done | bytes 32784 | tf_op jit(solution)/shard_map/reduce_scatter | solution.py:25
  210.9 2.0 multiply_reduce_fusion.2
  212.9 6.3 %all-reduce.1 = (f32[]{:T(128)}, f32[]{:T(128)}, f32[]{:T(128)}) all-reduce(f32[]{:T(128)} %get-tuple-element.26, f32[]{:T(128)} %get-tuple-element.22, f32[]{:T(128)} %get-tuple-element.18), channel_id=1, replica_groups=mesh['fs'=8,'tp'=4] {'tp'}, use_global_device_ids=true, to_apply=%region_2.0 | all-reduce | flops 3 | bytes 24 | tf_op jit(solution)/shard_map/psum | solution.py:75
  219.2 20.1 %all-reduce = (f32[]{:T(128)}, f32[]{:T(128)}, f32[]{:T(128)}) all-reduce(f32[]{:T(128)} %get-tuple-element.15, f32[]{:T(128)} %get-tuple-element.16, f32[]{:T(128)} %get-tuple-element.17), channel_id=1, replica_groups=mesh['fs'=8,'tp'=4] {'fs'}, use_global_device_ids=true, to_apply=%region_3.0 | all-reduce | flops 3 | bytes 24 | tf_op jit(solution)/shard_map/psum | solution.py:75
  240.0 2.3 subtract_convert_fusion.7
  243.0 32.4 %all_gather.20 = f32[256,512]{1,0:T(8,128)S(1)} all-gather(f32[32,512]{1,0:T(8,128)S(1)} %get-tuple-element.19), channel_id=1, replica_groups=mesh['fs'=8,'tp'=4] {'fs'}, dimensions={0}, use_global_device_ids=true | all-gather | bytes 589824 | tf_op jit(solution)/shard_map/all_gather | solution.py:41
  275.5 2.5 subtract_convert_fusion.6
  278.7 32.3 %all_gather.18 = f32[256,512]{1,0:T(8,128)S(1)} all-gather(f32[32,512]{1,0:T(8,128)S(1)} %get-tuple-element.27), channel_id=1, replica_groups=mesh['fs'=8,'tp'=4] {'fs'}, dimensions={0}, use_global_device_ids=true | all-gather | bytes 589824 | tf_op jit(solution)/shard_map/all_gather | solution.py:41
  311.0 2.3 subtract_convert_fusion.8
  313.3 34.7 %all-gather.8.cloned.1.call-done = bf16[2048,512]{1,0:T(8,128)(2,1)} async-done(((bf16[256,512]{1,0:T(8,128)(2,1)}), bf16[2048,512]{1,0:T(8,128)(2,1)}) %all-gather.8.cloned.1.call-update) | async-done | bytes 2097168 | tf_op jit(solution)/shard_map/all_gather | solution.py:82
  348.0 50.2 %all-gather.4.cloned.1.call-done = bf16[2048,512]{1,0:T(8,128)(2,1)} async-done(((bf16[256,512]{1,0:T(8,128)(2,1)}), bf16[2048,512]{1,0:T(8,128)(2,1)}) %all-gather.4.cloned.1.call-update) | async-done | bytes 2097168 | tf_op jit(solution)/shard_map/all_gather | solution.py:80
  398.2 3.2 copy.32
  401.4 1.3 copy.33
  (47 shorter events, 5.0 us)
Async XLA Ops:
  7.2 6.3 %copy-start = (bf16[2048,512]{1,0:T(8,128)(2,1)S(1)}, bf16[2048,512]{1,0:T(8,128)(2,1)}, u32[]{:S(2)}) copy-start(bf16[2048,512]{1,0:T(8,128)(2,1)} %param.19) | copy-start | bytes 6291460
  7.2 73.6 %reduce-scatter.6.cloned.1.call-start = ((), (), s32[]{:S(2)}) async-start(), calls=%async_computation.4 | async-start | bytes 294912 | tf_op jit(solution)/shard_map/reduce_scatter | solution.py:25
  14.3 1.6 copy-start.13
  15.8 130.0 %reduce-scatter.8.cloned.1.call-start = ((), (), s32[]{:S(2)}) async-start(), calls=%async_computation.5 | async-start | bytes 294912 | tf_op jit(solution)/shard_map/reduce_scatter | solution.py:25
  15.8 6.0 %copy-start.1 = (bf16[2048,512]{1,0:T(8,128)(2,1)S(1)}, bf16[2048,512]{1,0:T(8,128)(2,1)}, u32[]{:S(2)}) copy-start(bf16[2048,512]{1,0:T(8,128)(2,1)} %param.20) | copy-start | bytes 6291460
  22.6 1.5 copy-start.14
  24.1 186.8 %reduce-scatter.4.cloned.1.call-start = ((), (), s32[]{:S(2)}) async-start(), calls=%async_computation.3 | async-start | bytes 294912 | tf_op jit(solution)/shard_map/reduce_scatter | solution.py:25
  24.2 6.1 %copy-start.2 = (bf16[2048,512]{1,0:T(8,128)(2,1)S(1)}, bf16[2048,512]{1,0:T(8,128)(2,1)}, u32[]{:S(2)}) copy-start(bf16[2048,512]{1,0:T(8,128)(2,1)} %param.18) | copy-start | bytes 6291460
  31.0 49.8 %copy-start.7 = (f32[32,512]{1,0:T(8,128)S(1)}, f32[32,512]{1,0:T(8,128)}, u32[]{:S(2)}) copy-start(f32[32,512]{1,0:T(8,128)} %param.32) | copy-start | bytes 196612
  31.0 49.8 %copy-start.8 = (f32[32,512]{1,0:T(8,128)S(1)}, f32[32,512]{1,0:T(8,128)}, u32[]{:S(2)}) copy-start(f32[32,512]{1,0:T(8,128)} %param.29) | copy-start | bytes 196612
  31.0 114.8 %copy-start.9 = (f32[32,512]{1,0:T(8,128)S(1)}, f32[32,512]{1,0:T(8,128)}, u32[]{:S(2)}) copy-start(f32[32,512]{1,0:T(8,128)} %param.33) | copy-start | bytes 196612
  31.0 114.8 %copy-start.10 = (f32[32,512]{1,0:T(8,128)S(1)}, f32[32,512]{1,0:T(8,128)}, u32[]{:S(2)}) copy-start(f32[32,512]{1,0:T(8,128)} %param.30) | copy-start | bytes 196612
  31.0 179.8 %copy-start.11 = (f32[32,512]{1,0:T(8,128)S(1)}, f32[32,512]{1,0:T(8,128)}, u32[]{:S(2)}) copy-start(f32[32,512]{1,0:T(8,128)} %param.31) | copy-start | bytes 196612
  31.1 179.8 %copy-start.12 = (f32[32,512]{1,0:T(8,128)S(1)}, f32[32,512]{1,0:T(8,128)}, u32[]{:S(2)}) copy-start(f32[32,512]{1,0:T(8,128)} %param.28) | copy-start | bytes 196612
  32.5 207.4 %copy-start.5 = (f32[256,512]{1,0:T(8,128)S(1)}, f32[256,512]{1,0:T(8,128)}, u32[]{:S(2)}) copy-start(f32[256,512]{1,0:T(8,128)} %param.26) | copy-start | bytes 1572868
  32.5 280.8 %all-gather.6.cloned.1.call-start = ((), (), s32[]{:S(2)}) async-start(), calls=%async_computation.7 | async-start | bytes 2359296 | tf_op jit(solution)/shard_map/all_gather | solution.py:81
  242.2 68.8 %copy-start.6 = (f32[256,512]{1,0:T(8,128)S(1)}, f32[256,512]{1,0:T(8,128)}, u32[]{:S(2)}) copy-start(f32[256,512]{1,0:T(8,128)} %param.25) | copy-start | bytes 1572868
  242.3 105.8 %all-gather.8.cloned.1.call-start = ((), (), s32[]{:S(2)}) async-start(), calls=%async_computation.8 | async-start | bytes 2359296 | tf_op jit(solution)/shard_map/all_gather | solution.py:82
  278.0 120.3 %all-gather.4.cloned.1.call-start = ((), (), s32[]{:S(2)}) async-start(), calls=%async_computation.6 | async-start | bytes 2359296 | tf_op jit(solution)/shard_map/all_gather | solution.py:80
  398.2 3.2 copy-start.3
  401.4 2.3 copy-start.4
Sparse Core Ops, SparseCore 0:
  15.9 64.7 reduce-scatter.5
  84.6 61.1 reduce-scatter.7
  149.7 61.1 reduce-scatter.3
  242.4 54.5 all-gather.5
  299.6 48.4 all-gather.7
  350.6 47.6 all-gather.3
